TPU v7x, 32 devices: a whole 2x2x4 slice. The times are simulated.
32 devices in a mesh: grp: 2 (over x), ep: 16 (over z, y, core).
Axes of the slice: x: 2, y: 2, z: 4, core: 2. Of those that a mesh axis runs over, the one named last changes fastest.
Arguments:
- tokens: bfloat16 [2048, 2048], P(('grp', 'ep')), parts along dimension 0, may hold values from -6 to 6
- lengths: int32 [256], P(('grp', 'ep')), parts along dimension 0, may hold values from 1 to 8, 384 in all
- experts: int32 [2048, 2], P(('grp', 'ep')), parts along dimension 0, may hold values from 0 to 3, all different within a row; in each aligned block of 64 rows (0 to 63, 64 to 127, ...) at most 64 rows name the same one
- route_weights: float32 [2048, 2], P(('grp', 'ep')), parts along dimension 0, may hold values from 0.2 to 1
- gate_proj: bfloat16 [16, 2048, 1792], P('ep'), may hold values from -0.125 to 0.125
- up_proj: bfloat16 [16, 2048, 1792], P('ep'), may hold values from -0.125 to 0.125
- down_proj: bfloat16 [16, 1792, 2048], P('ep'), may hold values from -0.0625 to 0.0625
- norm_gain: float32 [2048], replicated, may hold values from 0.1 to 1.9
- norm_bias: float32 [2048], replicated, may hold values from -3 to 3
Outputs:
- mixed: bfloat16 [2048, 2048], P(('grp', 'ep')), parts along dimension 0
There are 2 independent parts, one for each index of `grp`. A program takes and returns all parts, laid end to end along the dimension named above; an argument that names none is the same for every part. Nothing has to cross between parts.
Inputs may be any that keep to these rules, and one draw needn't show every extreme that they name: Each row names 2 different experts; in the rows of one device (aligned blocks of 64 rows) no expert is named by more than 64 rows. Within each copy of the problem the 128 lengths sum to 384; the whole array, over all copies, sums to that times the number of copies.
All inputs are finite; a program needn't handle non-finite values. No bound on the sum of `lengths` on one device may be relied on, other than what follows from the above.
Results may differ from a plain program's by a relative error of at most 0.0021.
Values may be sent and summed in bfloat16 or wider, within the bound.
A program may use at most 128 MiB of HBM per device.

v0:
```python
import jax
import jax.numpy as jnp
from jax import lax
from jax.sharding import PartitionSpec as P

SPLIT = 4
TOP = 2
SPAN = 8
RESIDUAL_SCALE = 8.0**0.25
NORM_EPS = 1e-05


def layer_norm(values, norm_gain, norm_bias):
    center = values - jnp.mean(values, -1, keepdims=True)
    variance = jnp.mean(center * center, -1, keepdims=True)
    return center * lax.rsqrt(variance + NORM_EPS) * norm_gain + norm_bias


def expert_rows(picked, gate_proj, up_proj, down_proj):
    pre_gate = jnp.dot(picked, gate_proj[0], preferred_element_type=jnp.float32)
    pre_up = jnp.dot(picked, up_proj[0], preferred_element_type=jnp.float32)
    hidden = (jax.nn.silu(pre_gate) * pre_up).astype(jnp.bfloat16)
    return jnp.dot(hidden, down_proj[0], preferred_element_type=jnp.float32)


def local(
    tokens, lengths, experts, route_weights, gate_proj, up_proj, down_proj, norm_gain, norm_bias
):
    slot_count, width = tokens.shape
    axis_count = lax.axis_size("ep")
    capacity = 2 * slot_count * TOP * SPLIT // axis_count
    position = jnp.arange(slot_count, dtype=jnp.int32)
    alive_mask = position % SPAN < jnp.repeat(lengths, SPAN, total_repeat_length=slot_count)
    inputs = tokens.astype(jnp.float32)
    gathered = lax.all_gather(tokens, "ep", axis=0, tiled=True)
    all_experts, all_lengths = (
        lax.all_gather(experts, "ep", axis=0, tiled=True),
        lax.all_gather(lengths, "ep", axis=0, tiled=True),
    )
    all_weights = lax.all_gather(route_weights, "ep", axis=0, tiled=True)
    total_slots = gathered.shape[0]
    all_position = jnp.arange(total_slots, dtype=jnp.int32)
    all_alive = all_position % SPAN < jnp.repeat(all_lengths, SPAN, total_repeat_length=total_slots)
    own_expert = lax.axis_index("ep") // SPLIT
    hits = (all_experts == own_expert) & all_alive[:, None]
    chosen = hits.reshape(total_slots * TOP).astype(jnp.int32)
    order_rank = jnp.cumsum(chosen) - 1
    row_count = axis_count * capacity
    rows_index = jnp.arange(row_count, dtype=jnp.int32)
    picker = (order_rank[None, :] == rows_index[:, None]) & (chosen[None, :] == 1)
    flat_slot = jnp.repeat(all_position, TOP, total_repeat_length=total_slots * TOP)
    row_source = jnp.sum(jnp.where(picker, flat_slot[None, :], 0), axis=1)
    picked = jnp.take(gathered, row_source, axis=0)
    results = expert_rows(picked, gate_proj, up_proj, down_proj)
    rank_pairs = order_rank.reshape(total_slots, TOP)
    slot_row = jnp.sum(jnp.where(hits, rank_pairs, 0), axis=1)
    slot_weight = jnp.sum(jnp.where(hits, all_weights, 0.0), axis=1)
    spread_back = jnp.take(results, slot_row, axis=0) * slot_weight[:, None]
    branch = lax.psum_scatter(spread_back, "ep", scatter_dimension=0, tiled=True)
    normed = layer_norm(RESIDUAL_SCALE * inputs + branch, norm_gain, norm_bias)
    return jnp.where(alive_mask[:, None], normed, 0.0).astype(jnp.bfloat16)


def solution(mesh):
    in_specs = (
        P(("grp", "ep"), None),
        P(("grp", "ep")),
        P(("grp", "ep"), None),
        P(("grp", "ep"), None),
        P("ep", None, None),
        P("ep", None, None),
        P("ep", None, None),
        P(),
        P(),
    )
    out_specs = P(("grp", "ep"), None)
    return jax.shard_map(local, mesh=mesh, in_specs=in_specs, out_specs=out_specs, check_vma=False)
```

profile of v0, /device:TPU:0, one launch (start us, length us, event | category | flops | bytes accessed | tf_op | source)
XLA Modules:
  0.0 260.8 jit_solution(14044084314716863981)
XLA Ops:
  6.5 0.7 all-gather.4.cloned.1.call-update
  7.3 23.6 %all-gather = s32[16,64,2]{1,2,0:T(2,128)S(1)} all-gather(s32[1,64,2]{1,2,0:T(2,128)} %bitcast.52), channel_id=1, replica_groups=mesh['grp'=2,'ep'=16] {'ep'}, dimensions={0}, use_global_device_ids=true | all-gather | bytes 8704 | tf_op jit(solution)/shard_map/all_gather | solution.py:37
  31.0 1.2 dynamic-slice.18
  32.9 0.9 dynamic-update-slice.8
  33.8 7.1 %all-reduce = s32[128]{0:T(128)S(1)} all-reduce(s32[128]{0:T(128)S(1)} %dynamic-update-slice.8), channel_id=1, replica_groups=mesh['grp'=2,'ep'=16] {'ep'}, use_global_device_ids=true, to_apply=%add | all-reduce | flops 128 | bytes 1024
  40.9 0.8 add_add_fusion.1
  41.7 6.6 %gather_fusion = s32[1024]{0:T(1024)S(1)} fusion(s32[128]{0:T(128)S(1)} %all-reduce, s32[1024]{0:T(1024)S(1)} %broadcast_clamp_fusion.2), kind=kCustom, calls=%fused_computation | custom fusion | bytes 12288 | tf_op jit(solution)/shard_map/jit(_take)/gather | solution.py:43
  48.3 0.8 fusion.12
  49.9 0.5 reshape.354
  50.4 23.2 %all-gather.1 = f32[16,64,2]{1,2,0:T(2,128)S(1)} all-gather(f32[1,64,2]{1,2,0:T(2,128)} %bitcast.53), channel_id=1, replica_groups=mesh['grp'=2,'ep'=16] {'ep'}, dimensions={0}, use_global_device_ids=true | all-gather | bytes 8704 | tf_op jit(solution)/shard_map/all_gather | solution.py:40
  73.9 0.4 eq.44
  74.9 2.5 select_reduce_fusion
  77.5 11.7 %gather_fusion.1 = bf16[1024,2048]{1,0:T(8,128)(2,1)} fusion(bf16[1024,2048]{1,0:T(8,128)(2,1)} %all-gather.4.cloned.1.call-done, s32[1024]{0:T(1024)S(1)} %broadcast_clamp_fusion.1), kind=kCustom, calls=%fused_computation.1 | custom fusion | bytes 8392704 | tf_op jit(solution)/shard_map/jit(_take)/gather | solution.py:53
  89.3 13.9 %fusion.5 = f32[1024,1792]{1,0:T(8,128)} fusion(bf16[1,2048,1792]{2,1,0:T(8,128)(2,1)} %param.19, bf16[1024,2048]{1,0:T(8,128)(2,1)} %gather_fusion.1, pred[1024]{0:T(1024)(128)(4,1)S(1)} %compare_and_fusion), kind=kOutput, calls=%fused_computation.11 | convolution fusion | flops 7518289920 | bytes 18875392 | tf_op jit(solution)/shard_map/dot_general | solution.py:20
  103.1 26.9 %fusion.1 = f32[1024,2048]{1,0:T(8,128)} fusion(bf16[1,1792,2048]{2,1,0:T(8,128)(2,1)} %param.21, f32[1024,1792]{1,0:T(8,128)} %fusion.5, bf16[1,2048,1792]{2,1,0:T(8,128)(2,1)} %param.20, bf16[1024,2048]{1,0:T(8,128)(2,1)} %gather_fusion.1, pred[1024]{0:T(1024)(128)(4,1)S(1)} %compare_and_fusion), kind=kOutput, calls=%fused_computation.7 | convolution fusion | flops 15045492736 | bytes 34604032 | tf_op jit(solution)/shard_map/dot_general | solution.py:23
  130.1 12.5 %gather_fusion.2 = f32[1024,2048]{1,0:T(8,128)} fusion(f32[1024,2048]{1,0:T(8,128)} %fusion.1, s32[1024]{0:T(1024)S(1)} %broadcast_clamp_fusion), kind=kCustom, calls=%fused_computation.2 | custom fusion | bytes 16781312 | tf_op jit(solution)/shard_map/jit(_take)/gather | solution.py:58
  142.5 6.0 %select_multiply_fusion = f32[1024,2048]{1,0:T(8,128)} fusion(f32[1024,2048]{1,0:T(8,128)} %gather_fusion.2, f32[1024]{0:T(1024)S(1)} %select_reduce_fusion.1, pred[1024]{0:T(1024)(128)(4,1)S(1)} %compare_and_fusion.1), kind=kLoop, calls=%fused_computation.3 | loop fusion | flops 4194304 | bytes 16782336 | tf_op jit(solution)/shard_map/mul | solution.py:58
  148.6 0.5 copy-done.1
  149.1 0.7 fusion.22
  149.9 5.1 %fusion.16 = pred[64]{0:T(512)(128)(4,1)S(1)} fusion(pred[64]{0:T(512)(128)(4,1)S(1)} %copy-done.10, pred[64]{0:T(512)(128)(4,1)S(1)} %copy-done.9, pred[64]{0:T(512)(128)(4,1)S(1)} %copy-done.8, pred[64]{0:T(512)(128)(4,1)S(1)} %copy-done.7, pred[64]{0:T(512)(128)(4,1)S(1)} %copy-done.6, pred[64]{0:T(512)(128)(4,1)S(1)} %copy-done.5, ...), kind=kLoop, calls=%fused_computation.46 | loop fusion | flops 896 | bytes 544 | tf_op jit(solution)/shard_map/lt | solution.py:33
  154.9 94.5 %reduce-scatter.2.cloned.1.call-done = f32[64,2048]{1,0:T(8,128)} async-done(((f32[1024,2048]{1,0:T(8,128)}), f32[64,2048]{1,0:T(8,128)}) %reduce-scatter.2.cloned.1.call-update) | async-done | bytes 524304 | tf_op jit(solution)/shard_map/reduce_scatter | solution.py:59
  249.5 1.2 fusion.11
  250.7 1.3 multiply_reduce_fusion
  252.0 1.9 select_convert_fusion
  (55 shorter events, 2.2 us)
Async XLA Ops:
  6.5 71.0 %all-gather.4.cloned.1.call-start = ((), (), s32[]{:S(2)}) async-start(), calls=%async_computation.1 | async-start | bytes 4456448 | tf_op jit(solution)/shard_map/all_gather | solution.py:35
  7.3 242.2 %reduce-scatter.2.cloned.1.call-start = ((), (), s32[]{:S(2)}) async-start(), calls=%async_computation.2 | async-start | bytes 8912896 | tf_op jit(solution)/shard_map/reduce_scatter | solution.py:59
  148.5 0.7 copy-start.1
  148.5 1.3 copy-start.4
  148.5 1.3 copy-start.5
  148.5 1.3 copy-start.6
  148.5 1.3 copy-start.7
  148.5 1.3 copy-start.8
  148.5 1.3 copy-start.9
  148.5 1.3 copy-start.10
  148.6 100.9 %copy-start = (bf16[64,2048]{1,0:T(8,128)(2,1)S(1)}, bf16[64,2048]{1,0:T(8,128)(2,1)}, u32[]{:S(2)}) copy-start(bf16[64,2048]{1,0:T(8,128)(2,1)} %param.15) | copy-start | bytes 786436
  148.6 103.4 %copy-start.2 = (f32[2048]{0:T(1024)S(1)}, f32[2048]{0:T(1024)}, u32[]{:S(2)}) copy-start(f32[2048]{0:T(1024)} %param.23) | copy-start | bytes 24580
  148.6 103.4 %copy-start.3 = (f32[2048]{0:T(1024)S(1)}, f32[2048]{0:T(1024)}, u32[]{:S(2)}) copy-start(f32[2048]{0:T(1024)} %param.22) | copy-start | bytes 24580
Sparse Core Ops, SparseCore 0:
  9.5 53.3 all-gather.3
  148.7 100.6 reduce-scatter.1
where the time goes:
time: 261 us
  waiting for transfers between devices  95.3 us (37%)
  blocking collectives  53.9 us (21%)
  matrix products  40.8 us (16%)
  local copies, waits for them, and re-layouts  36.4 us (14%)
  other arithmetic  20 us (8%)
  between operations  14.3 us (5%)
    reduce_scatter x1, waiting for transfers between devices, local(): lax.psum_scatter(spread_back, 'ep', scatter_dimension=0, tiled=True)  94.5 us
    dot_general x1, matrix products, expert_rows(): return jnp.dot(hidden, down_proj[0], preferred_element_type=jnp.float32)  26.9 us
    all_gather x1, blocking collectives, local(): lax.all_gather(experts, 'ep', axis=0, tiled=True)  23.6 us
    all_gather x1, blocking collectives, local(): all_weights = lax.all_gather(route_weights, 'ep', axis=0, tiled=True)  23.2 us
    dot_general x1, matrix products, expert_rows(): pre_gate = jnp.dot(picked, gate_proj[0], preferred_element_type=jnp.float32)  13.9 us
    gather x1, local copies, waits for them, and re-layouts, local(): spread_back = jnp.take(results, slot_row, axis=0) * slot_weight[:, None]  12.5 us
    gather x1, local copies, waits for them, and re-layouts, local(): picked = jnp.take(gathered, row_source, axis=0)  11.7 us
    unnamed x1, blocking collectives  7.11 us
  transfers between devices with their start and end apart: 2, of which 1 were waited for; matrix products, arithmetic and copies ran while one was open for 8% of the time, Pallas kernels for 0%

commit v1 on v0

--- a/solution.py
+++ b/solution.py
@@ -37,7 +37,12 @@
         lax.all_gather(experts, "ep", axis=0, tiled=True),
         lax.all_gather(lengths, "ep", axis=0, tiled=True),
     )
-    all_weights = lax.all_gather(route_weights, "ep", axis=0, tiled=True)
+    ring = [route_weights]
+    for hop in range(15):
+        ring.append(lax.ppermute(ring[-1], "ep", [(dev, (dev + 1) % 16) for dev in range(16)]))
+    all_weights = jnp.roll(
+        jnp.concatenate(ring[::-1], axis=0), (lax.axis_index("ep") + 1) * ring[0].shape[0], axis=0
+    )
     total_slots = gathered.shape[0]
     all_position = jnp.arange(total_slots, dtype=jnp.int32)
     all_alive = all_position % SPAN < jnp.repeat(all_lengths, SPAN, total_repeat_length=total_slots)

time: 261 us -> 313 us (1.20)
  waiting for transfers between devices: 95.3 us -> 169 us
  blocking collectives: 53.9 us -> 30.2 us
    ppermute x0 -> x15, waiting for transfers between devices: none -> 73.9 us  [local(): lax.ppermute(ring[-1], 'ep', [(dev, (dev + 1) % 16) for dev in range(16)])]
    all_gather x1 -> x0, blocking collectives: 23.2 us -> none  [local(): all_weights = lax.all_gather(route_weights, 'ep', axis=0, tiled=True)]
  transfers between devices with their start and end apart: 2 -> 17, of which waited for: 1 -> 15; matrix products, arithmetic and copies ran while one was open for 8% -> 7% of each run, Pallas kernels for 0% -> 0%
where the time goes in v1:
time: 313 us; the launch traced here: 312 us
  waiting for transfers between devices  169 us (54%)
  matrix products  40.8 us (13%)
  local copies, waits for them, and re-layouts  37.1 us (12%)
  blocking collectives  30.2 us (10%)
  other arithmetic  19.9 us (6%)
  between operations  14.3 us (5%)
    reduce_scatter x1, waiting for transfers between devices, local(): lax.psum_scatter(spread_back, 'ep', scatter_dimension=0, tiled=True)  94.6 us
    ppermute x15, waiting for transfers between devices, local(): lax.ppermute(ring[-1], 'ep', [(dev, (dev + 1) % 16) for dev in range(16)])  73.9 us
    dot_general x1, matrix products, expert_rows(): return jnp.dot(hidden, down_proj[0], preferred_element_type=jnp.float32)  26.9 us
    all_gather x1, blocking collectives, local(): lax.all_gather(experts, 'ep', axis=0, tiled=True)  23 us
    dot_general x1, matrix products, expert_rows(): pre_gate = jnp.dot(picked, gate_proj[0], preferred_element_type=jnp.float32)  13.9 us
    gather x1, local copies, waits for them, and re-layouts, local(): spread_back = jnp.take(results, slot_row, axis=0) * slot_weight[:, None]  12.4 us
    gather x1, local copies, waits for them, and re-layouts, local(): picked = jnp.take(gathered, row_source, axis=0)  11.7 us
    unnamed x1, blocking collectives  7.26 us
  transfers between devices with their start and end apart: 17, of which 15 were waited for; matrix products, arithmetic and copies ran while one was open for 7% of the time, Pallas kernels for 0%

profile of v1, /device:TPU:0, one launch (start us, length us, event | category | flops | bytes accessed | tf_op | source)
XLA Modules:
  0.0 312.3 jit_solution(15416777731591066100)
XLA Ops:
  9.7 23.0 %all-gather = s32[16,64,2]{1,2,0:T(2,128)S(1)} all-gather(s32[1,64,2]{1,2,0:T(2,128)} %bitcast.49), channel_id=1, replica_groups=mesh['grp'=2,'ep'=16] {'ep'}, dimensions={0}, use_global_device_ids=true | all-gather | bytes 8704 | tf_op jit(solution)/shard_map/all_gather | solution.py:37
  34.4 7.3 %all-reduce = s32[128]{0:T(128)S(1)} all-reduce(s32[128]{0:T(128)S(1)} %dynamic-update-slice.8), channel_id=1, replica_groups=mesh['grp'=2,'ep'=16] {'ep'}, use_global_device_ids=true, to_apply=%add | all-reduce | flops 128 | bytes 1024
  41.6 6.6 %gather_fusion = s32[1024]{0:T(1024)S(1)} fusion(s32[128]{0:T(128)S(1)} %all-reduce, s32[1024]{0:T(1024)S(1)} %broadcast_clamp_fusion.2), kind=kCustom, calls=%fused_computation | custom fusion | bytes 12288 | tf_op jit(solution)/shard_map/jit(_take)/gather | solution.py:48
  49.1 4.8 %collective-permute-done.1 = f32[64,2]{0,1:T(2,128)S(1)} collective-permute-done((f32[64,2]{0,1:T(2,128)S(1)}, f32[64,2]{0,1:T(2,128)S(1)}, u32[]{:S(2)}, u32[]{:S(2)}) %collective-permute-start.1) | collective-permute-done | bytes 544 | tf_op jit(solution)/shard_map/ppermute | solution.py:42
  54.9 4.9 %collective-permute-done.2 = f32[64,2]{0,1:T(2,128)S(1)} collective-permute-done((f32[64,2]{0,1:T(2,128)S(1)}, f32[64,2]{0,1:T(2,128)S(1)}, u32[]{:S(2)}, u32[]{:S(2)}) %collective-permute-start.2) | collective-permute-done | bytes 544 | tf_op jit(solution)/shard_map/ppermute | solution.py:42
  59.9 5.6 %collective-permute-done.3 = f32[64,2]{0,1:T(2,128)S(1)} collective-permute-done((f32[64,2]{0,1:T(2,128)S(1)}, f32[64,2]{0,1:T(2,128)S(1)}, u32[]{:S(2)}, u32[]{:S(2)}) %collective-permute-start.3) | collective-permute-done | bytes 544 | tf_op jit(solution)/shard_map/ppermute | solution.py:42
  66.2 5.0 %collective-permute-done.4 = f32[64,2]{0,1:T(2,128)S(1)} collective-permute-done((f32[64,2]{0,1:T(2,128)S(1)}, f32[64,2]{0,1:T(2,128)S(1)}, u32[]{:S(2)}, u32[]{:S(2)}) %collective-permute-start.4) | collective-permute-done | bytes 544 | tf_op jit(solution)/shard_map/ppermute | solution.py:42
  73.7 3.2 %collective-permute-done.5 = f32[64,2]{0,1:T(2,128)S(1)} collective-permute-done((f32[64,2]{0,1:T(2,128)S(1)}, f32[64,2]{0,1:T(2,128)S(1)}, u32[]{:S(2)}, u32[]{:S(2)}) %collective-permute-start.5) | collective-permute-done | bytes 544 | tf_op jit(solution)/shard_map/ppermute | solution.py:42
  76.9 5.7 %collective-permute-done.6 = f32[64,2]{0,1:T(2,128)S(1)} collective-permute-done((f32[64,2]{0,1:T(2,128)S(1)}, f32[64,2]{0,1:T(2,128)S(1)}, u32[]{:S(2)}, u32[]{:S(2)}) %collective-permute-start.6) | collective-permute-done | bytes 544 | tf_op jit(solution)/shard_map/ppermute | solution.py:42
  83.4 4.9 %collective-permute-done.7 = f32[64,2]{0,1:T(2,128)S(1)} collective-permute-done((f32[64,2]{0,1:T(2,128)S(1)}, f32[64,2]{0,1:T(2,128)S(1)}, u32[]{:S(2)}, u32[]{:S(2)}) %collective-permute-start.7) | collective-permute-done | bytes 544 | tf_op jit(solution)/shard_map/ppermute | solution.py:42
  88.3 5.7 %collective-permute-done.8 = f32[64,2]{0,1:T(2,128)S(1)} collective-permute-done((f32[64,2]{0,1:T(2,128)S(1)}, f32[64,2]{0,1:T(2,128)S(1)}, u32[]{:S(2)}, u32[]{:S(2)}) %collective-permute-start.8) | collective-permute-done | bytes 544 | tf_op jit(solution)/shard_map/ppermute | solution.py:42
  94.0 5.7 %collective-permute-done.9 = f32[64,2]{0,1:T(2,128)S(1)} collective-permute-done((f32[64,2]{0,1:T(2,128)S(1)}, f32[64,2]{0,1:T(2,128)S(1)}, u32[]{:S(2)}, u32[]{:S(2)}) %collective-permute-start.9) | collective-permute-done | bytes 544 | tf_op jit(solution)/shard_map/ppermute | solution.py:42
  99.7 5.7 %collective-permute-done.10 = f32[64,2]{0,1:T(2,128)S(1)} collective-permute-done((f32[64,2]{0,1:T(2,128)S(1)}, f32[64,2]{0,1:T(2,128)S(1)}, u32[]{:S(2)}, u32[]{:S(2)}) %collective-permute-start.10) | collective-permute-done | bytes 544 | tf_op jit(solution)/shard_map/ppermute | solution.py:42
  105.4 5.7 %collective-permute-done.11 = f32[64,2]{0,1:T(2,128)S(1)} collective-permute-done((f32[64,2]{0,1:T(2,128)S(1)}, f32[64,2]{0,1:T(2,128)S(1)}, u32[]{:S(2)}, u32[]{:S(2)}) %collective-permute-start.11) | collective-permute-done | bytes 544 | tf_op jit(solution)/shard_map/ppermute | solution.py:42
  111.1 5.7 %collective-permute-done.12 = f32[64,2]{0,1:T(2,128)S(1)} collective-permute-done((f32[64,2]{0,1:T(2,128)S(1)}, f32[64,2]{0,1:T(2,128)S(1)}, u32[]{:S(2)}, u32[]{:S(2)}) %collective-permute-start.12) | collective-permute-done | bytes 544 | tf_op jit(solution)/shard_map/ppermute | solution.py:42
  116.8 5.7 %collective-permute-done.13 = f32[64,2]{0,1:T(2,128)S(1)} collective-permute-done((f32[64,2]{0,1:T(2,128)S(1)}, f32[64,2]{0,1:T(2,128)S(1)}, u32[]{:S(2)}, u32[]{:S(2)}) %collective-permute-start.13) | collective-permute-done | bytes 544 | tf_op jit(solution)/shard_map/ppermute | solution.py:42
  122.5 5.7 %collective-permute-done.14 = f32[64,2]{0,1:T(2,128)S(1)} collective-permute-done((f32[64,2]{0,1:T(2,128)S(1)}, f32[64,2]{0,1:T(2,128)S(1)}, u32[]{:S(2)}, u32[]{:S(2)}) %collective-permute-start.14) | collective-permute-done | bytes 544 | tf_op jit(solution)/shard_map/ppermute | solution.py:42
  129.2 11.7 %gather_fusion.1 = bf16[1024,2048]{1,0:T(8,128)(2,1)} fusion(bf16[1024,2048]{1,0:T(8,128)(2,1)} %all-gather.3.cloned.1.call-done, s32[1024]{0:T(1024)S(1)} %broadcast_clamp_fusion.1), kind=kCustom, calls=%fused_computation.1 | custom fusion | bytes 8392704 | tf_op jit(solution)/shard_map/jit(_take)/gather | solution.py:58
  140.9 13.9 %fusion.5 = f32[1024,1792]{1,0:T(8,128)} fusion(bf16[1,2048,1792]{2,1,0:T(8,128)(2,1)} %param.19, bf16[1024,2048]{1,0:T(8,128)(2,1)} %gather_fusion.1, pred[1024]{0:T(1024)(128)(4,1)S(1)} %compare_and_fusion), kind=kOutput, calls=%fused_computation.11 | convolution fusion | flops 7518289920 | bytes 18875392 | tf_op jit(solution)/shard_map/dot_general | solution.py:20
  154.8 26.9 %fusion.1 = f32[1024,2048]{1,0:T(8,128)} fusion(bf16[1,1792,2048]{2,1,0:T(8,128)(2,1)} %param.21, f32[1024,1792]{1,0:T(8,128)} %fusion.5, bf16[1,2048,1792]{2,1,0:T(8,128)(2,1)} %param.20, bf16[1024,2048]{1,0:T(8,128)(2,1)} %gather_fusion.1, pred[1024]{0:T(1024)(128)(4,1)S(1)} %compare_and_fusion), kind=kOutput, calls=%fused_computation.7 | convolution fusion | flops 15045492736 | bytes 34604032 | tf_op jit(solution)/shard_map/dot_general | solution.py:23
  181.7 12.4 %gather_fusion.2 = f32[1024,2048]{1,0:T(8,128)} fusion(f32[1024,2048]{1,0:T(8,128)} %fusion.1, s32[1024]{0:T(1024)S(1)} %broadcast_clamp_fusion), kind=kCustom, calls=%fused_computation.2 | custom fusion | bytes 16781312 | tf_op jit(solution)/shard_map/jit(_take)/gather | solution.py:63
  194.1 6.0 %select_multiply_fusion = f32[1024,2048]{1,0:T(8,128)} fusion(f32[1024,2048]{1,0:T(8,128)} %gather_fusion.2, f32[1024]{0:T(1024)S(1)} %select_reduce_fusion.1, pred[1024]{0:T(1024)(128)(4,1)S(1)} %compare_and_fusion.1), kind=kLoop, calls=%fused_computation.3 | loop fusion | flops 4194304 | bytes 16782336 | tf_op jit(solution)/shard_map/mul | solution.py:63
  201.4 5.0 %fusion.16 = pred[64]{0:T(512)(128)(4,1)S(1)} fusion(pred[64]{0:T(512)(128)(4,1)S(1)} %copy-done.10, pred[64]{0:T(512)(128)(4,1)S(1)} %copy-done.9, pred[64]{0:T(512)(128)(4,1)S(1)} %copy-done.8, pred[64]{0:T(512)(128)(4,1)S(1)} %copy-done.7, pred[64]{0:T(512)(128)(4,1)S(1)} %copy-done.6, pred[64]{0:T(512)(128)(4,1)S(1)} %copy-done.5, ...), kind=kLoop, calls=%fused_computation.46 | loop fusion | flops 896 | bytes 544 | tf_op jit(solution)/shard_map/lt | solution.py:33
  206.4 94.6 %reduce-scatter.2.cloned.1.call-done = f32[64,2048]{1,0:T(8,128)} async-done(((f32[1024,2048]{1,0:T(8,128)}), f32[64,2048]{1,0:T(8,128)}) %reduce-scatter.2.cloned.1.call-update) | async-done | bytes 524304 | tf_op jit(solution)/shard_map/reduce_scatter | solution.py:64
  (83 shorter events, 16.8 us)
Async XLA Ops:
  6.5 122.6 %all-gather.3.cloned.1.call-start = ((), (), s32[]{:S(2)}) async-start(), calls=%async_computation.1 | async-start | bytes 4456448 | tf_op jit(solution)/shard_map/all_gather | solution.py:35
  7.3 293.8 %reduce-scatter.2.cloned.1.call-start = ((), (), s32[]{:S(2)}) async-start(), calls=%async_computation.2 | async-start | bytes 8912896 | tf_op jit(solution)/shard_map/reduce_scatter | solution.py:64
  7.3 40.9 %collective-permute-start = (f32[64,2]{0,1:T(2,128)}, f32[64,2]{0,1:T(2,128)S(1)}, u32[]{:S(2)}, u32[]{:S(2)}) collective-permute-start(f32[64,2]{0,1:T(2,128)} %param.18), channel_id=1, source_target_pairs={{0,1},{1,2},{2,3},{3,4},{4,5},{5,6},{6,7},{7,8},{8,9},{9,10},{10,1... | collective-permute-start | bytes 1544 | tf_op jit(solution)/shard_map/ppermute | solution.py:42
  48.2 5.7 %collective-permute-start.1 = (f32[64,2]{0,1:T(2,128)S(1)}, f32[64,2]{0,1:T(2,128)S(1)}, u32[]{:S(2)}, u32[]{:S(2)}) collective-permute-start(f32[64,2]{0,1:T(2,128)S(1)} %collective-permute-done), channel_id=1, source_target_pairs={{0,1},{1,2},{2,3},{3,4},{4,5},{5,6},{6,7},{7,8},{8,9},{9,10},{10,1... | collective-permute-start | bytes 1544 | tf_op jit(solution)/shard_map/ppermute | solution.py:42
  54.0 5.8 %collective-permute-start.2 = (f32[64,2]{0,1:T(2,128)S(1)}, f32[64,2]{0,1:T(2,128)S(1)}, u32[]{:S(2)}, u32[]{:S(2)}) collective-permute-start(f32[64,2]{0,1:T(2,128)S(1)} %collective-permute-done.1), channel_id=1, source_target_pairs={{0,1},{1,2},{2,3},{3,4},{4,5},{5,6},{6,7},{7,8},{8,9},{9,10},{10,1... | collective-permute-start | bytes 1544 | tf_op jit(solution)/shard_map/ppermute | solution.py:42
  59.8 5.7 %collective-permute-start.3 = (f32[64,2]{0,1:T(2,128)S(1)}, f32[64,2]{0,1:T(2,128)S(1)}, u32[]{:S(2)}, u32[]{:S(2)}) collective-permute-start(f32[64,2]{0,1:T(2,128)S(1)} %collective-permute-done.2), channel_id=1, source_target_pairs={{0,1},{1,2},{2,3},{3,4},{4,5},{5,6},{6,7},{7,8},{8,9},{9,10},{10,1... | collective-permute-start | bytes 1544 | tf_op jit(solution)/shard_map/ppermute | solution.py:42
  65.5 5.7 %collective-permute-start.4 = (f32[64,2]{0,1:T(2,128)S(1)}, f32[64,2]{0,1:T(2,128)S(1)}, u32[]{:S(2)}, u32[]{:S(2)}) collective-permute-start(f32[64,2]{0,1:T(2,128)S(1)} %collective-permute-done.3), channel_id=1, source_target_pairs={{0,1},{1,2},{2,3},{3,4},{4,5},{5,6},{6,7},{7,8},{8,9},{9,10},{10,1... | collective-permute-start | bytes 1544 | tf_op jit(solution)/shard_map/ppermute | solution.py:42
  71.2 5.7 %collective-permute-start.5 = (f32[64,2]{0,1:T(2,128)S(1)}, f32[64,2]{0,1:T(2,128)S(1)}, u32[]{:S(2)}, u32[]{:S(2)}) collective-permute-start(f32[64,2]{0,1:T(2,128)S(1)} %collective-permute-done.4), channel_id=1, source_target_pairs={{0,1},{1,2},{2,3},{3,4},{4,5},{5,6},{6,7},{7,8},{8,9},{9,10},{10,1... | collective-permute-start | bytes 1544 | tf_op jit(solution)/shard_map/ppermute | solution.py:42
  76.9 5.7 %collective-permute-start.6 = (f32[64,2]{0,1:T(2,128)S(1)}, f32[64,2]{0,1:T(2,128)S(1)}, u32[]{:S(2)}, u32[]{:S(2)}) collective-permute-start(f32[64,2]{0,1:T(2,128)S(1)} %collective-permute-done.5), channel_id=1, source_target_pairs={{0,1},{1,2},{2,3},{3,4},{4,5},{5,6},{6,7},{7,8},{8,9},{9,10},{10,1... | collective-permute-start | bytes 1544 | tf_op jit(solution)/shard_map/ppermute | solution.py:42
  82.6 5.7 %collective-permute-start.7 = (f32[64,2]{0,1:T(2,128)S(1)}, f32[64,2]{0,1:T(2,128)S(1)}, u32[]{:S(2)}, u32[]{:S(2)}) collective-permute-start(f32[64,2]{0,1:T(2,128)S(1)} %collective-permute-done.6), channel_id=1, source_target_pairs={{0,1},{1,2},{2,3},{3,4},{4,5},{5,6},{6,7},{7,8},{8,9},{9,10},{10,1... | collective-permute-start | bytes 1544 | tf_op jit(solution)/shard_map/ppermute | solution.py:42
  88.3 5.7 %collective-permute-start.8 = (f32[64,2]{0,1:T(2,128)S(1)}, f32[64,2]{0,1:T(2,128)S(1)}, u32[]{:S(2)}, u32[]{:S(2)}) collective-permute-start(f32[64,2]{0,1:T(2,128)S(1)} %collective-permute-done.7), channel_id=1, source_target_pairs={{0,1},{1,2},{2,3},{3,4},{4,5},{5,6},{6,7},{7,8},{8,9},{9,10},{10,1... | collective-permute-start | bytes 1544 | tf_op jit(solution)/shard_map/ppermute | solution.py:42
  94.0 5.7 %collective-permute-start.9 = (f32[64,2]{0,1:T(2,128)S(1)}, f32[64,2]{0,1:T(2,128)S(1)}, u32[]{:S(2)}, u32[]{:S(2)}) collective-permute-start(f32[64,2]{0,1:T(2,128)S(1)} %collective-permute-done.8), channel_id=1, source_target_pairs={{0,1},{1,2},{2,3},{3,4},{4,5},{5,6},{6,7},{7,8},{8,9},{9,10},{10,1... | collective-permute-start | bytes 1544 | tf_op jit(solution)/shard_map/ppermute | solution.py:42
  99.7 5.7 %collective-permute-start.10 = (f32[64,2]{0,1:T(2,128)S(1)}, f32[64,2]{0,1:T(2,128)S(1)}, u32[]{:S(2)}, u32[]{:S(2)}) collective-permute-start(f32[64,2]{0,1:T(2,128)S(1)} %collective-permute-done.9), channel_id=1, source_target_pairs={{0,1},{1,2},{2,3},{3,4},{4,5},{5,6},{6,7},{7,8},{8,9},{9,10},{10,1... | collective-permute-start | bytes 1544 | tf_op jit(solution)/shard_map/ppermute | solution.py:42
  105.4 5.7 %collective-permute-start.11 = (f32[64,2]{0,1:T(2,128)S(1)}, f32[64,2]{0,1:T(2,128)S(1)}, u32[]{:S(2)}, u32[]{:S(2)}) collective-permute-start(f32[64,2]{0,1:T(2,128)S(1)} %collective-permute-done.10), channel_id=1, source_target_pairs={{0,1},{1,2},{2,3},{3,4},{4,5},{5,6},{6,7},{7,8},{8,9},{9,10},{10,1... | collective-permute-start | bytes 1544 | tf_op jit(solution)/shard_map/ppermute | solution.py:42
  111.1 5.7 %collective-permute-start.12 = (f32[64,2]{0,1:T(2,128)S(1)}, f32[64,2]{0,1:T(2,128)S(1)}, u32[]{:S(2)}, u32[]{:S(2)}) collective-permute-start(f32[64,2]{0,1:T(2,128)S(1)} %collective-permute-done.11), channel_id=1, source_target_pairs={{0,1},{1,2},{2,3},{3,4},{4,5},{5,6},{6,7},{7,8},{8,9},{9,10},{10,1... | collective-permute-start | bytes 1544 | tf_op jit(solution)/shard_map/ppermute | solution.py:42
  116.8 5.7 %collective-permute-start.13 = (f32[64,2]{0,1:T(2,128)S(1)}, f32[64,2]{0,1:T(2,128)S(1)}, u32[]{:S(2)}, u32[]{:S(2)}) collective-permute-start(f32[64,2]{0,1:T(2,128)S(1)} %collective-permute-done.12), channel_id=1, source_target_pairs={{0,1},{1,2},{2,3},{3,4},{4,5},{5,6},{6,7},{7,8},{8,9},{9,10},{10,1... | collective-permute-start | bytes 1544 | tf_op jit(solution)/shard_map/ppermute | solution.py:42
  122.5 5.7 %collective-permute-start.14 = (f32[64,2]{0,1:T(2,128)S(1)}, f32[64,2]{0,1:T(2,128)S(1)}, u32[]{:S(2)}, u32[]{:S(2)}) collective-permute-start(f32[64,2]{0,1:T(2,128)S(1)} %collective-permute-done.13), channel_id=1, source_target_pairs={{0,1},{1,2},{2,3},{3,4},{4,5},{5,6},{6,7},{7,8},{8,9},{9,10},{10,1... | collective-permute-start | bytes 1544 | tf_op jit(solution)/shard_map/ppermute | solution.py:42
  200.1 1.3 copy-start.6
  200.1 1.3 copy-start.7
  200.1 1.3 copy-start.8
  200.1 1.3 copy-start.9
  200.1 100.9 %copy-start = (bf16[64,2048]{1,0:T(8,128)(2,1)S(1)}, bf16[64,2048]{1,0:T(8,128)(2,1)}, u32[]{:S(2)}) copy-start(bf16[64,2048]{1,0:T(8,128)(2,1)} %param.15) | copy-start | bytes 786436
  200.1 103.4 %copy-start.2 = (f32[2048]{0:T(1024)S(1)}, f32[2048]{0:T(1024)}, u32[]{:S(2)}) copy-start(f32[2048]{0:T(1024)} %param.23) | copy-start | bytes 24580
  200.1 103.4 %copy-start.3 = (f32[2048]{0:T(1024)S(1)}, f32[2048]{0:T(1024)}, u32[]{:S(2)}) copy-start(f32[2048]{0:T(1024)} %param.22) | copy-start | bytes 24580
  (4 other events, 4.6 us)
Sparse Core Ops, SparseCore 0:
  9.5 53.2 all-gather.2
  200.3 100.6 reduce-scatter.1
